TPU v7x, 32 devices: a whole 2x2x4 slice. The times are simulated.
32 devices in a mesh: sp: 8 (over z, y), tp: 4 (over x, core).
Axes of the slice: x: 2, y: 2, z: 4, core: 2. Of those that a mesh axis runs over, the one named last changes fastest.
Arguments:
- queries: bfloat16 [3072, 2048], P('sp', 'tp'), may hold values from -6 to 6
- keys: bfloat16 [3072, 2048], P('sp', 'tp'), may hold values from -6 to 6
- values: bfloat16 [3072, 2048], P('sp', 'tp'), may hold values from -6 to 6
- gates: bfloat16 [3072, 2048], P('sp', 'tp'), may hold values from -8 to 8
- decay_pre: float32 [32, 3072], P('tp', 'sp'), may hold values from -18 to 3
- beta_pre: float32 [32, 3072], P('tp', 'sp'), may hold values from -10 to 3
- out_gain: float32 [64], replicated, may hold values from 0.1 to 1.9
- w_out: bfloat16 [2048, 2048], P('tp'), may hold values from -0.125 to 0.125
- stream: bfloat16 [3072, 2048], P(('sp', 'tp')), may hold values from -6 to 6
- norm_gain: float32 [2048], replicated, may hold values from 0.1 to 1.9
- w_gate: bfloat16 [2048, 5632], P('sp', 'tp'), may hold values from -0.125 to 0.125
- w_up: bfloat16 [2048, 5632], P('sp', 'tp'), may hold values from -0.125 to 0.125
- w_down: bfloat16 [5632, 2048], P('tp', 'sp'), may hold values from -0.078125 to 0.078125
Outputs:
- updated: bfloat16 [3072, 2048], P(('sp', 'tp'))
All inputs are finite; a program needn't handle non-finite values.
Results may differ from a plain program's by a relative error of at most 0.019.
Values may be sent and summed in bfloat16 or wider, within the bound.
A program may use at most 128 MiB of HBM per device.

v0:
```python
import jax
import jax.numpy as jnp
from jax import lax
from jax.sharding import PartitionSpec as P

HEAD_DIM = 64
BLOCK = 64


EPSILON = 1e-06
EXACT_PRECISION = lax.Precision.HIGHEST


def prefix(x, axis, combine, identity):
    size, index = (lax.axis_size(axis), lax.axis_index(axis))
    everything = jax.tree.map(
        lambda part, kind: lax.all_gather(part.astype(kind), axis), x, (jnp.bfloat16, jnp.bfloat16)
    )
    start = jax.tree.map(
        lambda part, zero: jnp.broadcast_to(jnp.asarray(zero, part.dtype), part.shape), x, identity
    )

    def hop(k, before):
        reached = k < index
        new = combine(
            before, jax.tree.map(lambda part, own: part[k].astype(own.dtype), everything, x)
        )
        return jax.tree.map(lambda a, b: jnp.where(reached, a, b), new, before)

    return lax.fori_loop(0, size, hop, start)


def unit_lower_inverse(lower_mat):
    span_len = lower_mat.shape[-1]
    identity = jnp.eye(span_len, dtype=jnp.float32)
    power = -lower_mat
    inverse = identity + power
    steps = 1
    while 1 << steps < span_len:
        power = jnp.einsum("...ij,...jk->...ik", power, power, precision=EXACT_PRECISION)
        inverse = jnp.einsum(
            "...ij,...jk->...ik", inverse, identity + power, precision=EXACT_PRECISION
        )
        steps = steps + 1
    return inverse


def prepare(queries, keys, values, beta_pre, decay_pre):
    length = queries.shape[0]
    heads = queries.shape[1] // HEAD_DIM

    def split_heads(arr):
        return arr.astype(jnp.float32).reshape(length, heads, HEAD_DIM)

    query_unit = jax.nn.silu(split_heads(queries))
    query_unit = query_unit * lax.rsqrt(
        jnp.sum(query_unit * query_unit, axis=-1, keepdims=True) + EPSILON
    )
    query_unit = (query_unit * HEAD_DIM ** (-0.5)).astype(jnp.bfloat16)
    key_unit = jax.nn.silu(split_heads(keys))
    key_unit = (
        key_unit * lax.rsqrt(jnp.sum(key_unit * key_unit, axis=-1, keepdims=True) + EPSILON)
    ).astype(jnp.bfloat16)
    value_act = jax.nn.silu(split_heads(values))
    strength = jax.nn.sigmoid(beta_pre)
    log_decay = -jax.nn.softplus(decay_pre)
    nblocks = length // BLOCK

    def blocked(arr):
        return arr.reshape(nblocks, BLOCK, heads, HEAD_DIM).transpose(0, 2, 1, 3)

    def blocked_rates(arr):
        return arr.reshape(heads, nblocks, BLOCK).transpose(1, 0, 2)

    return (
        blocked(query_unit),
        blocked(key_unit),
        blocked(value_act),
        blocked_rates(strength),
        blocked_rates(log_decay),
    )


def block_terms(query_blk, key_blk, value_blk, strength_blk, decay_blk):
    span_len = query_blk.shape[-2]
    query_f = query_blk.astype(jnp.float32)
    key_f = key_blk.astype(jnp.float32)
    cumulative = jnp.cumsum(decay_blk, axis=-1)
    row_ids = jnp.arange(span_len)[:, None]
    col_ids = jnp.arange(span_len)[None, :]
    inclusive = row_ids >= col_ids
    strict = row_ids > col_ids
    decay_mat = jnp.exp(
        jnp.where(inclusive, cumulative[..., :, None] - cumulative[..., None, :], -jnp.inf)
    )
    key_inner = jnp.einsum(
        "...id,...jd->...ij", key_blk, key_blk, preferred_element_type=jnp.float32
    )
    lower_mat = jnp.where(strict, strength_blk[..., :, None] * key_inner * decay_mat, 0.0)
    key_strong = key_f * strength_blk[..., None]
    right_side = jnp.concatenate(
        [value_blk * strength_blk[..., None], key_strong * jnp.exp(cumulative)[..., None]], axis=-1
    )
    solved = jnp.einsum(
        "...ij,...jk->...ik", unit_lower_inverse(lower_mat), right_side, precision=EXACT_PRECISION
    )
    width = value_blk.shape[-1]
    update_values = solved[..., :width]
    update_keys = solved[..., width:]
    query_inner = jnp.einsum(
        "...id,...jd->...ij", query_blk, key_blk, preferred_element_type=jnp.float32
    )
    inside_span = jnp.where(inclusive, query_inner * decay_mat, 0.0)
    final_decay = cumulative[..., -1:]
    key_attenuated = key_f * jnp.exp(final_decay - cumulative)[..., None]
    query_attenuated = query_f * jnp.exp(cumulative)[..., None]
    return (update_values, update_keys, inside_span, query_attenuated, key_attenuated, final_decay)


def advance(matrix_state, terms):
    update_values, update_keys, inside_span, query_attenuated, key_attenuated, final_decay = terms
    value_corrected = update_values - jnp.einsum(
        "jod,jdg->jog", update_keys, matrix_state, precision=EXACT_PRECISION
    )
    output_result = jnp.einsum(
        "jod,jdg->jog", query_attenuated, matrix_state, precision=EXACT_PRECISION
    ) + jnp.einsum("oyn,onk->oyk", inside_span, value_corrected, precision=EXACT_PRECISION)
    matrix_state = matrix_state * jnp.exp(final_decay)[..., None] + jnp.einsum(
        "lyq,lyf->lqf", key_attenuated, value_corrected, precision=EXACT_PRECISION
    )
    return (matrix_state, output_result)


def compose(carry, items):
    trans_mat, offset_mat = carry
    update_keys, update_values, key_attenuated, final_decay = items
    heads = update_keys.shape[0]
    identity = jnp.broadcast_to(jnp.eye(HEAD_DIM, dtype=jnp.float32), (heads, HEAD_DIM, HEAD_DIM))
    step_trans = jnp.exp(final_decay)[..., None] * identity - jnp.einsum(
        "hck,hcl->hkl", key_attenuated, update_keys, precision=EXACT_PRECISION
    )
    stride_displacement = jnp.einsum(
        "lyq,lyf->lqf", key_attenuated, update_values, precision=EXACT_PRECISION
    )
    new_trans = jnp.einsum("hkl,hlm->hkm", step_trans, trans_mat, precision=EXACT_PRECISION)
    new_offset = (
        jnp.einsum("hkl,hlm->hkm", step_trans, offset_mat, precision=EXACT_PRECISION)
        + stride_displacement
    )
    return ((new_trans, new_offset), None)


def chain(earlier, later):
    joined_trans = jnp.einsum("hkl,hlm->hkm", later[0], earlier[0], precision=EXACT_PRECISION)
    joined_offset = (
        jnp.einsum("hkl,hlm->hkm", later[0], earlier[1], precision=EXACT_PRECISION) + later[1]
    )
    return (joined_trans, joined_offset)


def finish(outputs, gates, out_gain):
    length = gates.shape[0]
    heads = gates.shape[1] // HEAD_DIM
    heads_out = outputs.transpose(0, 2, 1, 3).reshape(length, heads, HEAD_DIM)
    heads_out = heads_out * lax.rsqrt(
        jnp.mean(heads_out * heads_out, axis=-1, keepdims=True) + EPSILON
    )
    heads_out = heads_out * out_gain
    gated = heads_out * jax.nn.silu(gates.astype(jnp.float32).reshape(length, heads, HEAD_DIM))
    return gated.reshape(length, heads * HEAD_DIM).astype(jnp.bfloat16)


def per_device(
    queries,
    keys,
    values,
    gates,
    decay_pre,
    beta_pre,
    out_gain,
    w_out,
    stream,
    norm_gain,
    w_gate,
    w_up,
    w_down,
):
    blocks = prepare(queries, keys, values, beta_pre, decay_pre)
    terms = block_terms(*blocks)
    update_values, update_keys, inside_span, query_attenuated, key_attenuated, final_decay = terms
    heads = update_keys.shape[1]
    identity = jnp.broadcast_to(jnp.eye(HEAD_DIM, dtype=jnp.float32), (heads, HEAD_DIM, HEAD_DIM))
    zero_state = jnp.zeros((heads, HEAD_DIM, HEAD_DIM), jnp.float32)
    (trans_mat, offset_mat), _ = lax.scan(
        compose, (identity, zero_state), (update_keys, update_values, key_attenuated, final_decay)
    )
    earlier_part = prefix((trans_mat, offset_mat), "sp", chain, (identity, zero_state))
    _, outputs = lax.scan(advance, earlier_part[1], terms)
    mixed_heads = finish(outputs, gates, out_gain)
    head_block = lax.all_to_all(mixed_heads, "tp", split_axis=0, concat_axis=1, tiled=True)
    out_whole = lax.all_gather(w_out, "tp", axis=0, tiled=True)
    projected = jnp.dot(head_block, out_whole, preferred_element_type=jnp.float32)
    middle = (stream.astype(jnp.float32) + projected).astype(jnp.bfloat16)
    middle_f = middle.astype(jnp.float32)
    normed = middle_f * lax.rsqrt(jnp.mean(middle_f * middle_f, axis=-1, keepdims=True) + EPSILON)
    normed = (normed * norm_gain).astype(jnp.bfloat16)
    span_rows = lax.all_gather(normed, "tp", axis=0, tiled=True)
    gate_hidden = jnp.dot(
        span_rows,
        lax.all_gather(w_gate, "sp", axis=0, tiled=True),
        preferred_element_type=jnp.float32,
    )
    up_hidden = jnp.dot(
        span_rows,
        lax.all_gather(w_up, "sp", axis=0, tiled=True),
        preferred_element_type=jnp.float32,
    )
    hidden = (jax.nn.silu(gate_hidden) * up_hidden).astype(jnp.bfloat16)
    channel_term = jnp.dot(
        hidden, lax.all_gather(w_down, "sp", axis=1, tiled=True), preferred_element_type=jnp.float32
    )
    channel_sum = lax.psum_scatter(
        channel_term.astype(jnp.bfloat16), "tp", scatter_dimension=0, tiled=True
    ).astype(jnp.float32)
    return (middle_f + 0.5 * channel_sum).astype(jnp.bfloat16)


def solution(mesh):
    return jax.shard_map(
        per_device,
        mesh=mesh,
        in_specs=(
            P("sp", "tp"),
            P("sp", "tp"),
            P("sp", "tp"),
            P("sp", "tp"),
            P("tp", "sp"),
            P("tp", "sp"),
            P(),
            P("tp", None),
            P(("sp", "tp"), None),
            P(),
            P("sp", "tp"),
            P("sp", "tp"),
            P("tp", "sp"),
        ),
        out_specs=P(("sp", "tp"), None),
        check_vma=False,
    )
```

profile of v0, /device:TPU:0, one launch (start us, length us, event | category | flops | bytes accessed | tf_op | source)
XLA Modules:
  0.0 467.2 jit_solution(12672921094007981784)
XLA Ops:
  8.3 1.8 reshape.144
  13.1 2.7 copy.76
  19.4 5.9 %fusion.46 = (f32[6,8,64,64]{3,2,1,0:T(8,128)S(1)}, bf16[6,64,8,64]{3,1,2,0:T(8,128)(2,1)S(1)}, f32[6,8,64,64]{3,2,1,0:T(8,128)}, f32[6,8,64,64]{3,2,1,0:T(8,128)S(1)}) fusion(f32[6,8,64]{2,1,0:T(8,128)S(1)} %get-tuple-element.343, f32[6,8,64]{2,1,0:T(8,128)S(1)} %copy.68, f32[6,64,8]{1,2,0:T(8,128)S(1)} %copy.67, f32[6,64,8,64]{3,1,2,0:T(8,128)} %copy.66, ...), kind=kLoop, calls=%fused_computation.60 | loop fusion | flops 4521984 | bytes 5160960 | tf_op jit(solution)/shard_map/mul | solution.py:102
  25.3 2.4 multiply_select_fusion
  28.6 1.8 fusion.81
  32.2 1.8 fusion.59
  39.2 2.0 fusion.55
  46.5 1.9 fusion.47
  48.4 2.2 fusion.79
  52.2 1.9 copy.72
  54.3 21.5 %while.43 = (s32[]{:T(128)}, f32[8,64,64]{2,1,0:T(8,128)S(1)}, f32[8,64,64]{2,1,0:T(8,128)S(1)}, f32[6,8,1]{1,2,0:T(1,128)S(1)}, f32[6,8,64,64]{2,3,1,0:T(8,128)...) while((s32[]{:T(128)}, f32[8,64,64]{2,1,0:T(8,128)S(1)}, ...), condition=%wide.region_3.4_spmd.clone.clone, body=%wide.region_2.3_spmd.clone.sunk.clone | while | flops 100802560 | bytes 2673307 | solution.py:194
  75.7 40.9 %all-gather = bf16[64,64,64]{2,1,0:T(8,128)(2,1)} all-gather(bf16[8,64,64]{2,1,0:T(8,128)(2,1)S(1)} %convert_element_type.98), channel_id=2, replica_groups=mesh['sp'=8,'tp'=4] {'sp'}, dimensions={0}, use_global_device_ids=true | all-gather | bytes 589824 | tf_op jit(solution)/shard_map/all_gather | solution.py:17
  116.7 38.9 %all-gather.1 = bf16[64,64,64]{2,1,0:T(8,128)(2,1)} all-gather(bf16[8,64,64]{2,1,0:T(8,128)(2,1)S(1)} %convert_element_type.99), channel_id=3, replica_groups=mesh['sp'=8,'tp'=4] {'sp'}, dimensions={0}, use_global_device_ids=true | all-gather | bytes 589824 | tf_op jit(solution)/shard_map/all_gather | solution.py:17
  155.5 10.7 %while.44 = (s32[]{:T(128)}, f32[8,64,64]{2,1,0:T(8,128)S(1)}, s32[]{:T(128)}, bf16[8,8,64,64]{3,2,1,0:T(8,128)(2,1)}, bf16[8,8,64,64]{3,2,1,0:T(8,128)(2,1)}) while((s32[]{:T(128)}, f32[8,64,64]{2,1,0:T(8,128)S(1)}, s32[]{:T(128)}, bf16[8,8,64,64]{3,2,1,0:T(8,128)(2,1)}, bf16[8,8,64,64]{3,2,1,0:T(8,128)(2,1)}) %tuple.113), condition=%wide.region_5.6_spmd.clone.clone, body=%wide.region_4.5_spmd.clone.sunk.clone | while | flops 25329668 | bytes 1182287 | solution.py:30
  166.3 27.7 %while.42 = (s32[]{:T(128)}, f32[8,64,64]{2,1,0:T(8,128)S(1)}, f32[6,8,64,64]{3,2,1,0:T(8,128)S(1)}, f32[6,8,1]{1,2,0:T(1,128)S(1)}, f32[6,8,64,64]{2,3,1,0:T(8,...) while((s32[]{:T(128)}, f32[8,64,64]{2,1,0:T(8,128)S(1)}, ...), condition=%wide.region_8.9_spmd.clone, body=%wide.region_7.8_spmd.sunk.clone | while | flops 100794368 | bytes 3280037 | solution.py:198
  198.2 10.2 %all_to_all.19 = bf16[4,96,512]{2,1,0:T(8,128)(2,1)S(1)} all-to-all(bf16[4,96,512]{2,1,0:T(8,128)(2,1)S(1)} %bitcast.177), channel_id=1, replica_groups=mesh['sp'=8,'tp'=4] {'tp'}, dimensions={0} | all-to-all | bytes 786432 | tf_op jit(solution)/shard_map/all_to_all | solution.py:200
  208.5 5.0 %multiply_reduce_fusion.1 = (f32[96]{0:T(128)S(1)}, f32[96,2048]{1,0:T(8,128)S(1)}) fusion(bf16[96,2048]{1,0:T(8,128)(2,1)S(1)} %bitcast.173, bf16[2048,2048]{1,0:T(8,128)(2,1)} %all-gather.8.cloned.1.call-done, bf16[96,2048]{1,0:T(8,128)(2,1)S(1)} %copy-done.7), kind=kOutput, calls=%fused_computation.95 | convolution fusion | flops 806485888 | bytes 9961856 | tf_op jit(solution)/shard_map/dot_general | solution.py:202
  215.7 17.2 %all-gather.10.cloned.1.call-done = bf16[384,2048]{1,0:T(8,128)(2,1)} async-done(((bf16[96,2048]{1,0:T(8,128)(2,1)}), bf16[384,2048]{1,0:T(8,128)(2,1)}) %all-gather.10.cloned.1.call-update) | async-done | bytes 1572880 | tf_op jit(solution)/shard_map/all_gather | solution.py:207
  232.9 7.2 %fusion.86 = f32[384,1408]{1,0:T(8,128)} fusion(bf16[384,2048]{1,0:T(8,128)(2,1)} %all-gather.10.cloned.1.call-done, bf16[2048,1408]{1,0:T(8,128)(2,1)} %all-gather.12.cloned.1.call-done), kind=kOutput, calls=%fused_computation.126 | convolution fusion | flops 2214592512 | bytes 9502720 | tf_op jit(solution)/shard_map/dot_general | solution.py:208
  240.1 87.2 %all-gather.14.cloned.1.call-done = bf16[2048,1408]{1,0:T(8,128)(2,1)} async-done(((bf16[256,1408]{1,0:T(8,128)(2,1)}), bf16[2048,1408]{1,0:T(8,128)(2,1)}) %all-gather.14.cloned.1.call-update) | async-done | bytes 5767184 | tf_op jit(solution)/shard_map/all_gather | solution.py:215
  327.3 93.2 %all-gather.16.cloned.1.call-done = bf16[1408,2048]{1,0:T(8,128)(2,1)} async-done(((bf16[1408,256]{1,0:T(8,128)(2,1)}), bf16[1408,2048]{1,0:T(8,128)(2,1)}) %all-gather.16.cloned.1.call-update) | async-done | bytes 5767184 | tf_op jit(solution)/shard_map/all_gather | solution.py:220
  420.5 11.2 %convolution_convert_fusion = bf16[384,2048]{1,0:T(8,128)(2,1)} fusion(bf16[1408,2048]{1,0:T(8,128)(2,1)} %all-gather.16.cloned.1.call-done, bf16[384,2048]{1,0:T(8,128)(2,1)S(1)} %copy-done.12, bf16[2048,1408]{1,0:T(8,128)(2,1)} %all-gather.14.cloned.1.call-done, f32[384,1408]{1,0:T(8,128)} %fusion.86), kind=kOutput, calls=%fused_computation.54 | convolution fusion | flops 4433215488 | bytes 16842752 | tf_op jit(solution)/shard_map/dot_general | solution.py:219
  431.7 26.4 %reduce-scatter.2.cloned.1.call-done = bf16[96,2048]{1,0:T(8,128)(2,1)} async-done(((bf16[384,2048]{1,0:T(8,128)(2,1)}), bf16[96,2048]{1,0:T(8,128)(2,1)}) %reduce-scatter.2.cloned.1.call-update) | async-done | bytes 393232 | tf_op jit(solution)/shard_map/reduce_scatter | solution.py:222
  458.1 1.8 add_convert_fusion
  (182 shorter events, 88.1 us)
Async XLA Ops:
  6.5 1.5 copy-start.3
  6.5 202.0 %all-gather.8.cloned.1.call-start = ((), (), s32[]{:S(2)}) async-start(), calls=%async_computation.2 | async-start | bytes 10485760 | tf_op jit(solution)/shard_map/all_gather | solution.py:201
  7.3 208.4 %all-gather.12.cloned.1.call-start = ((), (), s32[]{:S(2)}) async-start(), calls=%async_computation.4 | async-start | bytes 6488064 | tf_op jit(solution)/shard_map/all_gather | solution.py:210
  8.0 224.9 %all-gather.10.cloned.1.call-start = ((), (), s32[]{:S(2)}) async-start(), calls=%async_computation.3 | async-start | bytes 1966080 | tf_op jit(solution)/shard_map/all_gather | solution.py:207
  8.3 2.1 copy-start.4
  10.6 0.8 copy-start.8
  16.0 1.7 copy-start.9
  16.0 1.8 copy-start.5
  17.6 1.8 copy-start
  116.7 49.6 %copy-start.1 = (f32[6,8,64,64]{3,2,1,0:T(8,128)S(1)}, f32[6,8,64,64]{3,2,1,0:T(8,128)}, u32[]{:S(2)}) copy-start(f32[6,8,64,64]{3,2,1,0:T(8,128)} %custom-call.2) | copy-start | bytes 2359300
  196.7 0.7 copy-start.11
  196.7 1.1 copy-start.2
  196.7 1.2 copy-start.6
  198.0 10.5 %copy-start.7 = (bf16[96,2048]{1,0:T(8,128)(2,1)S(1)}, bf16[96,2048]{1,0:T(8,128)(2,1)}, u32[]{:S(2)}) copy-start(bf16[96,2048]{1,0:T(8,128)(2,1)} %param.27) | copy-start | bytes 1179652
  208.5 5.0 %copy-start.10 = (f32[2048]{0:T(1024)S(1)}, f32[2048]{0:T(1024)}, u32[]{:S(2)}) copy-start(f32[2048]{0:T(1024)} %param.28) | copy-start | bytes 24580
  214.4 112.8 %all-gather.14.cloned.1.call-start = ((), (), s32[]{:S(2)}) async-start(), calls=%async_computation.5 | async-start | bytes 6488064 | tf_op jit(solution)/shard_map/all_gather | solution.py:215
  215.0 205.5 %all-gather.16.cloned.1.call-start = ((), (), s32[]{:S(2)}) async-start(), calls=%async_computation.6 | async-start | bytes 6488064 | tf_op jit(solution)/shard_map/all_gather | solution.py:220
  215.6 242.5 %reduce-scatter.2.cloned.1.call-start = ((), (), s32[]{:S(2)}) async-start(), calls=%async_computation.7 | async-start | bytes 1966080 | tf_op jit(solution)/shard_map/reduce_scatter | solution.py:222
  232.9 187.6 %copy-start.12 = (bf16[384,2048]{1,0:T(8,128)(2,1)S(1)}, bf16[384,2048]{1,0:T(8,128)(2,1)}, u32[]{:S(2)}) copy-start(bf16[384,2048]{1,0:T(8,128)(2,1)} %all-gather.10.cloned.1.call-done) | copy-start | bytes 4718596
Sparse Core Ops, SparseCore 0:
  8.9 60.9 all-gather.7
  72.1 116.8 all-gather.11
  214.6 18.2 all-gather.9
  234.9 92.3 all-gather.13
  329.1 91.2 all-gather.15
  431.8 26.2 reduce-scatter.1
where the time goes:
time: 472 us; the launch traced here: 467 us
  waiting for transfers between devices  227 us (48%)
  matrix products  105 us (22%)
  blocking collectives  90 us (19%)
  local copies, waits for them, and re-layouts  17.2 us (4%)
  between operations  14.4 us (3%)
  other arithmetic  13.1 us (3%)
    all_gather x1, waiting for transfers between devices, per_device(): lax.all_gather(w_down, 'sp', axis=1, tiled=True)  93.2 us
    all_gather x1, waiting for transfers between devices, per_device(): lax.all_gather(w_up, 'sp', axis=0, tiled=True)  87.2 us
    all_gather x2, blocking collectives, prefix(): lax.all_gather(part.astype(kind), axis)  79.8 us
    reduce_scatter x1, waiting for transfers between devices, per_device(): lax.psum_scatter(channel_term.astype(jnp.bfloat16), 'tp', scatter_dimensi...  26.4 us
    all_gather x1, waiting for transfers between devices, per_device(): span_rows = lax.all_gather(normed, 'tp', axis=0, tiled=True)  17.2 us
    dot_general x1, matrix products, per_device(): jnp.dot(hidden, lax.all_gather(w_down, 'sp', axis=1, tiled=True), preferr...  11.2 us
    all_to_all x1, blocking collectives, per_device(): lax.all_to_all(mixed_heads, 'tp', split_axis=0, concat_axis=1, tiled=True)  10.2 us
    dot_general x8, matrix products, chain(): jnp.einsum('hkl,hlm->hkm', later[0], earlier[1], precision=EXACT_PRECISION)  10 us
  transfers between devices with their start and end apart: 6, of which 4 were waited for; matrix products, arithmetic and copies ran while one was open for 26% of the time, Pallas kernels for 0%

commit v1 on v0

v1 whole, which is shorter than its diff:
```python
import functools

import jax
import jax.numpy as jnp
from jax import lax
from jax.experimental import pallas as pl
from jax.experimental.pallas import tpu as pltpu
from jax.sharding import PartitionSpec as P

HEAD_DIM = 64
EPSILON = 1e-06
EXACT_PRECISION = lax.Precision.HIGHEST
CHUNK = 128
PAIR = 2 * HEAD_DIM


def split_dot(left, right, dims):
    high = left.astype(jnp.bfloat16)
    low = (left - high.astype(jnp.float32)).astype(jnp.bfloat16)
    return dot(high, right, dims) + dot(low, right, dims)


def dot(left, right, dims):
    return lax.dot_general(
        left.astype(jnp.bfloat16),
        right.astype(jnp.bfloat16),
        (dims, ((), ())),
        preferred_element_type=jnp.float32,
    )


NN = ((1,), (0,))
NT = ((1,), (1,))
TN = ((0,), (0,))


def exact_dot(left, right, dims):
    return lax.dot_general(
        left, right, (dims, ((), ())), precision=EXACT_PRECISION, preferred_element_type=jnp.float32
    )


def silu(x):
    return x / (1.0 + jnp.exp(-x))


def iotas(rows, columns):
    return (
        lax.broadcasted_iota(jnp.int32, (rows, columns), 0),
        lax.broadcasted_iota(jnp.int32, (rows, columns), 1),
    )


def lower_inverse(lower, row_ids, col_ids):
    small = 16
    near = jnp.where(row_ids // small == col_ids // small, lower, 0.0)
    power = -near
    rest = power
    size = 2
    while size < small:
        power = dot(power, power, NN)
        rest = rest + power + dot(rest, power, NN)
        size *= 2
    size = small
    while size < lower.shape[0]:
        off = jnp.where(
            (row_ids // (2 * size) == col_ids // (2 * size)) & (row_ids // size != col_ids // size),
            lower,
            0.0,
        )
        half = off + dot(off, rest, NN)
        rest = rest - half - dot(rest, half, NN)
        size *= 2
    return rest


def mixer_kernel(q_ref, k_ref, v_ref, beta_ref, decay_ref, state_ref, local_ref, reach_ref):
    length, width = q_ref.shape
    pairs = width // PAIR
    row_ids, col_ids = iotas(CHUNK, CHUNK)
    inclusive = row_ids >= col_ids
    strict = row_ids > col_ids
    eye = (row_ids == col_ids).astype(jnp.float32)
    lower_ones = inclusive.astype(jnp.float32)
    same_half = (row_ids // HEAD_DIM == col_ids // HEAD_DIM).astype(jnp.bfloat16)
    first = col_ids < HEAD_DIM
    own = (first, jnp.logical_not(first))
    states = [
        [jnp.where(row_ids // HEAD_DIM == 1 - side, eye, 0.0) for side in range(2)]
        for _ in range(pairs)
    ]
    for chunk in range(length // CHUNK):
        rows = pl.ds(chunk * CHUNK, CHUNK)
        log_decay = -jax.nn.softplus(decay_ref[:, rows])
        strength = jax.nn.sigmoid(beta_ref[:, rows])
        cum_col = exact_dot(lower_ones, log_decay, NT)
        cum_row = exact_dot(log_decay, lower_ones, NT)
        strength_col = exact_dot(eye, strength, NT)
        grow_col = jnp.exp(cum_col)
        final_row = cum_col[CHUNK - 1 : CHUNK, :]
        fade_col = jnp.exp(final_row - cum_col)
        final_exp = jnp.exp(final_row)
        for pair in range(pairs):
            lanes = pl.ds(pair * PAIR, PAIR)

            def unit(ref):
                x = silu(ref[rows, lanes].astype(jnp.float32))
                total = split_dot(x * x, same_half, NN)
                return x * lax.rsqrt(total + EPSILON)

            query = (unit(q_ref) * HEAD_DIM ** (-0.5)).astype(jnp.bfloat16)
            key = unit(k_ref).astype(jnp.bfloat16)
            value = silu(v_ref[rows, lanes].astype(jnp.float32))
            query_turned = pltpu.roll(query.astype(jnp.float32), HEAD_DIM, 1)
            key_turned = pltpu.roll(key.astype(jnp.float32), HEAD_DIM, 1)
            outs = []
            for side in range(2):
                head = 2 * pair + side
                mine = own[side]
                col = slice(head, head + 1)
                cum = cum_col[:, col]
                decay_mat = jnp.exp(
                    jnp.where(inclusive, cum - cum_row[head : head + 1, :], -1e30)
                )
                masked = jnp.where(mine, key, jnp.zeros_like(key))
                key_inner = dot(masked, key, NT)
                query_inner = dot(query, masked, NT)
                lower = jnp.where(strict, strength_col[:, col] * key_inner * decay_mat, 0.0)
                right_side = strength_col[:, col] * jnp.where(
                    mine, value, key_turned * grow_col[:, col]
                )
                rest = lower_inverse(lower, row_ids, col_ids)
                solved = right_side + dot(rest, right_side, NN)
                state = states[pair][side]
                corrected = jnp.where(mine, solved, 0.0) - dot(
                    jnp.where(mine, 0.0, solved), state, NN
                )
                inside = query_inner * decay_mat
                result = dot(query_turned * grow_col[:, col], state, NN) + dot(
                    inside, corrected, NN
                )
                key_fading = jnp.where(mine, 0.0, key_turned * fade_col[:, col])
                states[pair][side] = state * final_exp[:, col] + dot(key_fading, corrected, TN)
                outs.append(result)
            local_ref[rows, lanes] = jnp.where(first, outs[0], outs[1])
            reach_ref[rows, lanes] = jnp.where(first, outs[1], outs[0]).astype(jnp.bfloat16)
    for pair in range(pairs):
        state_ref[pair] = (states[pair][0] + states[pair][1]).astype(jnp.bfloat16)


def mixer(queries, keys, values, beta_pre, decay_pre):
    length, width = queries.shape
    pairs = width // PAIR
    return pl.pallas_call(
        mixer_kernel,
        name="mixer",
        out_shape=(
            jax.ShapeDtypeStruct((pairs, PAIR, PAIR), jnp.bfloat16),
            jax.ShapeDtypeStruct((length, width), jnp.float32),
            jax.ShapeDtypeStruct((length, width), jnp.bfloat16),
        ),
        in_specs=[pl.BlockSpec(memory_space=pltpu.VMEM)] * 5,
        out_specs=(pl.BlockSpec(memory_space=pltpu.VMEM),) * 3,
        cost_estimate=pl.CostEstimate(
            flops=60 * length * PAIR * PAIR * pairs, bytes_accessed=8 * length * width, transcendentals=0
        ),
    )(queries, keys, values, beta_pre, decay_pre)


def finish_kernel(size, every_ref, local_ref, reach_ref, gates_ref, gain_ref, out_ref):
    length, width = local_ref.shape
    pairs = width // PAIR
    index = lax.axis_index("sp")
    row_ids, col_ids = iotas(PAIR, PAIR)
    same = row_ids // HEAD_DIM == col_ids // HEAD_DIM
    same_half = same.astype(jnp.bfloat16)

    def hop(step, before):
        reached = step < index
        after = []
        for pair in range(pairs):
            item = every_ref[step, pair]
            trans = jnp.where(same, item, jnp.zeros_like(item))
            offset = jnp.where(same, 0.0, item.astype(jnp.float32))
            high = before[pair].astype(jnp.bfloat16)
            low = (before[pair] - high.astype(jnp.float32)).astype(jnp.bfloat16)
            new = offset + dot(trans, high, NN) + dot(trans, low, NN)
            after.append(jnp.where(reached, new, before[pair]))
        return tuple(after)

    start = tuple(jnp.zeros((PAIR, PAIR), jnp.float32) for _ in range(pairs))
    earlier = lax.fori_loop(0, size - 1, hop, start)
    for pair in range(pairs):
        lanes = pl.ds(pair * PAIR, PAIR)
        heads_out = local_ref[:, lanes] + dot(reach_ref[:, lanes], earlier[pair], NN)
        mean = split_dot(heads_out * heads_out, same_half, NN) * (1.0 / HEAD_DIM)
        heads_out = heads_out * lax.rsqrt(mean + EPSILON) * gain_ref[...]
        gated = heads_out * silu(gates_ref[:, lanes].astype(jnp.float32))
        out_ref[:, lanes] = gated.astype(jnp.bfloat16)


def finish(every, local, reach, gates, out_gain):
    length, width = local.shape
    return pl.pallas_call(
        functools.partial(finish_kernel, every.shape[0]),
        name="finish",
        out_shape=jax.ShapeDtypeStruct((length, width), jnp.bfloat16),
        in_specs=[pl.BlockSpec(memory_space=pltpu.VMEM)] * 5,
        out_specs=pl.BlockSpec(memory_space=pltpu.VMEM),
        cost_estimate=pl.CostEstimate(
            flops=4 * length * width * PAIR, bytes_accessed=8 * length * width, transcendentals=0
        ),
    )(every, local, reach, gates, jnp.concatenate([out_gain, out_gain])[None, :])


def per_device(
    queries,
    keys,
    values,
    gates,
    decay_pre,
    beta_pre,
    out_gain,
    w_out,
    stream,
    norm_gain,
    w_gate,
    w_up,
    w_down,
):
    state, local, reach = mixer(queries, keys, values, beta_pre, decay_pre)
    every = lax.all_gather(state, "sp")
    mixed_heads = finish(every, local, reach, gates, out_gain)
    head_block = lax.all_to_all(mixed_heads, "tp", split_axis=0, concat_axis=1, tiled=True)
    out_whole = lax.all_gather(w_out, "tp", axis=0, tiled=True)
    projected = jnp.dot(head_block, out_whole, preferred_element_type=jnp.float32)
    middle = (stream.astype(jnp.float32) + projected).astype(jnp.bfloat16)
    middle_f = middle.astype(jnp.float32)
    normed = middle_f * lax.rsqrt(jnp.mean(middle_f * middle_f, axis=-1, keepdims=True) + EPSILON)
    normed = (normed * norm_gain).astype(jnp.bfloat16)
    span_rows = lax.all_gather(normed, "tp", axis=0, tiled=True)
    gate_hidden = jnp.dot(
        span_rows,
        lax.all_gather(w_gate, "sp", axis=0, tiled=True),
        preferred_element_type=jnp.float32,
    )
    up_hidden = jnp.dot(
        span_rows,
        lax.all_gather(w_up, "sp", axis=0, tiled=True),
        preferred_element_type=jnp.float32,
    )
    hidden = (jax.nn.silu(gate_hidden) * up_hidden).astype(jnp.bfloat16)
    channel_term = jnp.dot(
        hidden, lax.all_gather(w_down, "sp", axis=1, tiled=True), preferred_element_type=jnp.float32
    )
    channel_sum = lax.psum_scatter(
        channel_term.astype(jnp.bfloat16), "tp", scatter_dimension=0, tiled=True
    ).astype(jnp.float32)
    return (middle_f + 0.5 * channel_sum).astype(jnp.bfloat16)


def solution(mesh):
    return jax.shard_map(
        per_device,
        mesh=mesh,
        in_specs=(
            P("sp", "tp"),
            P("sp", "tp"),
            P("sp", "tp"),
            P("sp", "tp"),
            P("tp", "sp"),
            P("tp", "sp"),
            P(),
            P("tp", None),
            P(("sp", "tp"), None),
            P(),
            P("sp", "tp"),
            P("sp", "tp"),
            P("tp", "sp"),
        ),
        out_specs=P(("sp", "tp"), None),
        check_vma=False,
    )
```

time: 472 us -> 506 us (1.072)
  waiting for transfers between devices: 227 us -> 397 us
  matrix products: 105 us -> 23.4 us
  blocking collectives: 90 us -> 15.1 us
  Pallas kernels: 0 us -> 52.9 us
  local copies, waits for them, and re-layouts: 17.2 us -> 0.04 us
  other arithmetic: 13.1 us -> 3.38 us
    all_gather x1, waiting for transfers between devices: 0.02 us -> 85.2 us  [per_device(): lax.all_gather(w_gate, 'sp', axis=0, tiled=True)]
    dot_general x69 -> x0, matrix products: 81.3 us -> none  [the longest x8 10 us: chain(): jnp.einsum('hkl,hlm->hkm', later[0], earlier[1], precision=EXACT_PRECISION)]
    all_gather x2 -> x0, blocking collectives: 79.8 us -> none  [prefix(): lax.all_gather(part.astype(kind), axis)]
    pallas_call x0 -> x2, Pallas kernels: none -> 52.9 us  [the longest x1 47.9 us: mixer(): pl.pallas_call(mixer_kernel, name='mixer', out_shape=(jax.ShapeDtypeStruc...]
    all_gather x1, waiting for transfers between devices: 0.02 us -> 42.4 us  [per_device(): out_whole = lax.all_gather(w_out, 'tp', axis=0, tiled=True)]
    all_gather x0 -> x1, waiting for transfers between devices: none -> 41 us  [per_device(): every = lax.all_gather(state, 'sp')]
    reshape x8 -> x0, local copies, waits for them, and re-layouts: 9.54 us -> none  [the longest x5 8.11 us: split_heads(): return arr.astype(jnp.float32).reshape(length, heads, HEAD_DIM)]
    mul x2 -> x0, other arithmetic: 7.52 us -> none  [the longest x1 5.9 us: block_terms(): key_strong * jnp.exp(cumulative)[..., None]]
  transfers between devices with their start and end apart: 6 -> 7, of which waited for: 4 -> 7; matrix products, arithmetic and copies ran while one was open for 26% -> 3% of each run, Pallas kernels for 0% -> 1%
where the time goes in v1:
time: 506 us
  waiting for transfers between devices  397 us (78%)
  Pallas kernels  52.9 us (10%)
  matrix products  23.4 us (5%)
  blocking collectives  15.1 us (3%)
  between operations  13.5 us (3%)
    all_gather x1, waiting for transfers between devices, per_device(): lax.all_gather(w_down, 'sp', axis=1, tiled=True)  93.2 us
    all_gather x1, waiting for transfers between devices, per_device(): lax.all_gather(w_up, 'sp', axis=0, tiled=True)  87.2 us
    all_gather x1, waiting for transfers between devices, per_device(): lax.all_gather(w_gate, 'sp', axis=0, tiled=True)  85.2 us
    pallas_call x1, Pallas kernels, mixer(): pl.pallas_call(mixer_kernel, name='mixer', out_shape=(jax.ShapeDtypeStruc...  47.9 us
    all_gather x1, waiting for transfers between devices, per_device(): out_whole = lax.all_gather(w_out, 'tp', axis=0, tiled=True)  42.4 us
    all_gather x1, waiting for transfers between devices, per_device(): every = lax.all_gather(state, 'sp')  41 us
    reduce_scatter x1, waiting for transfers between devices, per_device(): lax.psum_scatter(channel_term.astype(jnp.bfloat16), 'tp', scatter_dimensi...  26.4 us
    all_gather x1, waiting for transfers between devices, per_device(): span_rows = lax.all_gather(normed, 'tp', axis=0, tiled=True)  19.3 us
  transfers between devices with their start and end apart: 7, of which 7 were waited for; matrix products, arithmetic and copies ran while one was open for 3% of the time, Pallas kernels for 1%

profile of v1, /device:TPU:0, one launch (start us, length us, event | category | flops | bytes accessed | tf_op | source)
XLA Modules:
  0.0 505.8 jit_solution(12358302015596073854)
XLA Ops:
  6.5 47.9 %mixer.1 = (bf16[4,128,128]{2,1,0:T(8,128)(2,1)}, f32[384,512]{1,0:T(8,128)}, bf16[384,512]{1,0:T(8,128)(2,1)}) custom-call(bf16[384,512]{1,0:T(8,128)(2,1)} %q_ref.1, bf16[384,512]{1,0:T(8,128)(2,1)} %k_ref.1, bf16[384,512]{1,0:T(8,128)(2,1)} %v_ref.1, f32[8,384]{1,0:T(8,128)} %beta_ref.1, f32[8,384]{1,0:T(8,128)} %decay_ref.1), custom_call_target="tpu_custom_call" | custom-call | flops 1509949440 | bytes 1572864 | tf_op jit(solution)/shard_map/mixer/pallas_call | solution.py:154
  54.5 0.0 all-gather.8.cloned.1.call-start
  54.5 0.7 all-gather.8.cloned.1.call-update
  55.3 0.7 all-gather.12.cloned.1.call-update
  56.0 0.0 all-gather.10.cloned.1.call-start
  56.0 0.6 maximum_bitcast_fusion.gain_ref
  56.7 41.0 %all-gather.18.cloned.1.call-done = bf16[32,128,128]{2,1,0:T(8,128)(2,1)} async-done(((bf16[4,128,128]{2,1,0:T(8,128)(2,1)}), bf16[32,128,128]{2,1,0:T(8,128)(2,1)}) %all-gather.18.cloned.1.call-update) | async-done | bytes 1048592 | tf_op jit(solution)/shard_map/all_gather | solution.py:232
  97.7 5.0 finish.1
  102.6 15.1 %all_to_all.19 = bf16[4,96,512]{2,1,0:T(8,128)(2,1)S(1)} all-to-all(bf16[4,96,512]{2,1,0:T(8,128)(2,1)} %bitcast.15), channel_id=1, replica_groups=mesh['sp'=8,'tp'=4] {'tp'}, dimensions={0} | all-to-all | bytes 786432 | tf_op jit(solution)/shard_map/all_to_all | solution.py:234
  117.8 42.4 %all-gather.8.cloned.1.call-done = bf16[2048,2048]{1,0:T(8,128)(2,1)} async-done(((bf16[512,2048]{1,0:T(8,128)(2,1)}), bf16[2048,2048]{1,0:T(8,128)(2,1)}) %all-gather.8.cloned.1.call-update) | async-done | bytes 8388624 | tf_op jit(solution)/shard_map/all_gather | solution.py:235
  160.2 5.0 multiply_reduce_fusion
  165.2 0.9 multiply_convert_fusion
  166.2 0.0 all-gather.14.cloned.1.call-start
  166.2 0.5 all-gather.14.cloned.1.call-update
  166.8 0.5 all-gather.16.cloned.1.call-update
  167.3 0.0 reduce-scatter.2.cloned.1.call-start
  167.4 85.2 %all-gather.12.cloned.1.call-done = bf16[2048,1408]{1,0:T(8,128)(2,1)} async-done(((bf16[256,1408]{1,0:T(8,128)(2,1)}), bf16[2048,1408]{1,0:T(8,128)(2,1)}) %all-gather.12.cloned.1.call-update) | async-done | bytes 5767184 | tf_op jit(solution)/shard_map/all_gather | solution.py:244
  252.6 19.3 %all-gather.10.cloned.1.call-done = bf16[384,2048]{1,0:T(8,128)(2,1)} async-done(((bf16[96,2048]{1,0:T(8,128)(2,1)}), bf16[384,2048]{1,0:T(8,128)(2,1)}) %all-gather.10.cloned.1.call-update) | async-done | bytes 1572880 | tf_op jit(solution)/shard_map/all_gather | solution.py:241
  271.8 7.2 %fusion.4 = f32[384,1408]{1,0:T(8,128)} fusion(bf16[384,2048]{1,0:T(8,128)(2,1)} %all-gather.10.cloned.1.call-done, bf16[2048,1408]{1,0:T(8,128)(2,1)} %all-gather.12.cloned.1.call-done), kind=kOutput, calls=%fused_computation.12 | convolution fusion | flops 2214592512 | bytes 9502720 | tf_op jit(solution)/shard_map/dot_general | solution.py:242
  279.0 87.2 %all-gather.14.cloned.1.call-done = bf16[2048,1408]{1,0:T(8,128)(2,1)} async-done(((bf16[256,1408]{1,0:T(8,128)(2,1)}), bf16[2048,1408]{1,0:T(8,128)(2,1)}) %all-gather.14.cloned.1.call-update) | async-done | bytes 5767184 | tf_op jit(solution)/shard_map/all_gather | solution.py:249
  366.2 93.2 %all-gather.16.cloned.1.call-done = bf16[1408,2048]{1,0:T(8,128)(2,1)} async-done(((bf16[1408,256]{1,0:T(8,128)(2,1)}), bf16[1408,2048]{1,0:T(8,128)(2,1)}) %all-gather.16.cloned.1.call-update) | async-done | bytes 5767184 | tf_op jit(solution)/shard_map/all_gather | solution.py:254
  459.5 11.2 %convolution_convert_fusion = bf16[384,2048]{1,0:T(8,128)(2,1)} fusion(bf16[1408,2048]{1,0:T(8,128)(2,1)} %all-gather.16.cloned.1.call-done, bf16[384,2048]{1,0:T(8,128)(2,1)S(1)} %copy-done.2, bf16[2048,1408]{1,0:T(8,128)(2,1)} %all-gather.14.cloned.1.call-done, f32[384,1408]{1,0:T(8,128)} %fusion.4), kind=kOutput, calls=%fused_computation.2 | convolution fusion | flops 4433215488 | bytes 16842752 | tf_op jit(solution)/shard_map/dot_general | solution.py:253
  470.7 26.4 %reduce-scatter.2.cloned.1.call-done = bf16[96,2048]{1,0:T(8,128)(2,1)} async-done(((bf16[384,2048]{1,0:T(8,128)(2,1)}), bf16[96,2048]{1,0:T(8,128)(2,1)}) %reduce-scatter.2.cloned.1.call-update) | async-done | bytes 393232 | tf_op jit(solution)/shard_map/reduce_scatter | solution.py:256
  497.1 1.8 add_convert_fusion
  (16 shorter events, 0.2 us)
Async XLA Ops:
  6.5 91.1 %all-gather.18.cloned.1.call-start = ((), (), s32[]{:S(2)}) async-start(), calls=%async_computation.8 | async-start | bytes 1179648 | tf_op jit(solution)/shard_map/all_gather | solution.py:232
  54.5 1.6 copy-start.3
  54.5 105.7 %all-gather.8.cloned.1.call-start = ((), (), s32[]{:S(2)}) async-start(), calls=%async_computation.2 | async-start | bytes 10485760 | tf_op jit(solution)/shard_map/all_gather | solution.py:235
  55.3 197.3 %all-gather.12.cloned.1.call-start = ((), (), s32[]{:S(2)}) async-start(), calls=%async_computation.4 | async-start | bytes 6488064 | tf_op jit(solution)/shard_map/all_gather | solution.py:244
  56.0 215.8 %all-gather.10.cloned.1.call-start = ((), (), s32[]{:S(2)}) async-start(), calls=%async_computation.3 | async-start | bytes 1966080 | tf_op jit(solution)/shard_map/all_gather | solution.py:241
  97.7 62.6 %copy-start = (bf16[96,2048]{1,0:T(8,128)(2,1)S(1)}, bf16[96,2048]{1,0:T(8,128)(2,1)}, u32[]{:S(2)}) copy-start(bf16[96,2048]{1,0:T(8,128)(2,1)} %param.21) | copy-start | bytes 1179652
  160.2 5.0 copy-start.1
  166.2 200.0 %all-gather.14.cloned.1.call-start = ((), (), s32[]{:S(2)}) async-start(), calls=%async_computation.5 | async-start | bytes 6488064 | tf_op jit(solution)/shard_map/all_gather | solution.py:249
  166.8 292.7 %all-gather.16.cloned.1.call-start = ((), (), s32[]{:S(2)}) async-start(), calls=%async_computation.6 | async-start | bytes 6488064 | tf_op jit(solution)/shard_map/all_gather | solution.py:254
  167.3 329.7 %reduce-scatter.2.cloned.1.call-start = ((), (), s32[]{:S(2)}) async-start(), calls=%async_computation.7 | async-start | bytes 1966080 | tf_op jit(solution)/shard_map/reduce_scatter | solution.py:256
  271.8 187.6 %copy-start.2 = (bf16[384,2048]{1,0:T(8,128)(2,1)S(1)}, bf16[384,2048]{1,0:T(8,128)(2,1)}, u32[]{:S(2)}) copy-start(bf16[384,2048]{1,0:T(8,128)(2,1)} %all-gather.10.cloned.1.call-done) | copy-start | bytes 4718596
Sparse Core Ops, SparseCore 0:
  54.6 42.9 all-gather.17
  99.2 60.9 all-gather.7
  162.4 90.1 all-gather.11
  254.0 17.7 all-gather.9
  273.9 92.3 all-gather.13
  368.1 91.2 all-gather.15
  470.8 26.2 reduce-scatter.1

commit v2 on v1

--- a/solution.py
+++ b/solution.py
@@ -6,6 +6,7 @@
 from jax.experimental import pallas as pl
 from jax.experimental.pallas import tpu as pltpu
 from jax.sharding import PartitionSpec as P
+
 
 HEAD_DIM = 64
 EPSILON = 1e-06
@@ -162,13 +163,13 @@
         in_specs=[pl.BlockSpec(memory_space=pltpu.VMEM)] * 5,
         out_specs=(pl.BlockSpec(memory_space=pltpu.VMEM),) * 3,
         cost_estimate=pl.CostEstimate(
-            flops=60 * length * PAIR * PAIR * pairs, bytes_accessed=8 * length * width, transcendentals=0
+            flops=2000 * length * PAIR * PAIR * pairs, bytes_accessed=8 * length * width, transcendentals=0
         ),
     )(queries, keys, values, beta_pre, decay_pre)
 
 
 def finish_kernel(size, every_ref, local_ref, reach_ref, gates_ref, gain_ref, out_ref):
-    length, width = local_ref.shape
+    _, width = local_ref.shape
     pairs = width // PAIR
     index = lax.axis_index("sp")
     row_ids, col_ids = iotas(PAIR, PAIR)
@@ -213,7 +214,42 @@
     )(every, local, reach, gates, jnp.concatenate([out_gain, out_gain])[None, :])
 
 
-def per_device(
+def exchange_gather(part, axis):
+    size = lax.axis_size(axis)
+    pieces = {0: part}
+    bits = [1 << i for i in range(1, size.bit_length() - 1)] + [1]
+    for bit in bits:
+        pairs = [(i, i ^ bit) for i in range(size)]
+        for held in list(pieces):
+            pieces[held ^ bit] = lax.ppermute(pieces[held], axis, pairs)
+    return [pieces[m] for m in range(size)]
+
+
+def place_kernel(middle_ref, sums_ref, out_ref):
+    size, index = lax.axis_size("sp"), lax.axis_index("sp")
+    width = out_ref.shape[1] // size
+    for owner in range(size):
+        lanes = pl.ds(owner * width, width)
+        start = (index ^ owner) * width
+        if width % 128 == 0:
+            start = pl.multiple_of(start, 128)
+        block = sums_ref[:, pl.ds(start, width)].astype(jnp.float32)
+        out_ref[:, lanes] = (middle_ref[:, lanes].astype(jnp.float32) + 0.5 * block).astype(
+            jnp.bfloat16
+        )
+
+
+def place(middle, sums):
+    return pl.pallas_call(
+        place_kernel,
+        name="place",
+        out_shape=jax.ShapeDtypeStruct(middle.shape, jnp.bfloat16),
+        in_specs=[pl.BlockSpec(memory_space=pltpu.VMEM)] * 2,
+        out_specs=pl.BlockSpec(memory_space=pltpu.VMEM),
+    )(middle, sums)
+
+
+def layer(
     queries,
     keys,
     values,
@@ -228,40 +264,68 @@
     w_up,
     w_down,
 ):
+    n_tp, tp = lax.axis_size("tp"), lax.axis_index("tp")
+    gate_whole = lax.all_gather(w_gate, "sp", axis=0, tiled=True)
+    up_whole = lax.all_gather(w_up, "sp", axis=0, tiled=True)
+    outs = [w_out]
+    for shift in range(1, n_tp):
+        ring = [(i, (i + shift) % n_tp) for i in range(n_tp)]
+        outs.append(lax.ppermute(w_out, "tp", ring))
+    downs = exchange_gather(w_down, "sp")
+
     state, local, reach = mixer(queries, keys, values, beta_pre, decay_pre)
-    every = lax.all_gather(state, "sp")
+    parts = 2
+    step = state.shape[0] // parts
+    every = jnp.concatenate(
+        [lax.all_gather(state[i * step : (i + 1) * step], "sp") for i in range(parts)], axis=1
+    )
     mixed_heads = finish(every, local, reach, gates, out_gain)
-    head_block = lax.all_to_all(mixed_heads, "tp", split_axis=0, concat_axis=1, tiled=True)
-    out_whole = lax.all_gather(w_out, "tp", axis=0, tiled=True)
-    projected = jnp.dot(head_block, out_whole, preferred_element_type=jnp.float32)
+    rows = stream.shape[0]
+    head_block = lax.all_to_all(
+        mixed_heads.reshape(n_tp, rows, mixed_heads.shape[1]), "tp", split_axis=0, concat_axis=0
+    )
+    projected = 0.0
+    for shift in range(n_tp):
+        owner = lax.rem(tp + n_tp - shift, n_tp)
+        block = lax.dynamic_index_in_dim(head_block, owner, axis=0, keepdims=False)
+        projected = projected + jnp.dot(block, outs[shift], preferred_element_type=jnp.float32)
     middle = (stream.astype(jnp.float32) + projected).astype(jnp.bfloat16)
     middle_f = middle.astype(jnp.float32)
     normed = middle_f * lax.rsqrt(jnp.mean(middle_f * middle_f, axis=-1, keepdims=True) + EPSILON)
     normed = (normed * norm_gain).astype(jnp.bfloat16)
-    span_rows = lax.all_gather(normed, "tp", axis=0, tiled=True)
-    gate_hidden = jnp.dot(
-        span_rows,
-        lax.all_gather(w_gate, "sp", axis=0, tiled=True),
-        preferred_element_type=jnp.float32,
-    )
-    up_hidden = jnp.dot(
-        span_rows,
-        lax.all_gather(w_up, "sp", axis=0, tiled=True),
-        preferred_element_type=jnp.float32,
-    )
+    span_rows = jnp.zeros((n_tp * rows, normed.shape[1]), normed.dtype)
+    span_rows = lax.dynamic_update_slice_in_dim(span_rows, normed, tp * rows, axis=0)
+    for shift in range(1, n_tp):
+        ring = [(i, (i + shift) % n_tp) for i in range(n_tp)]
+        moved = lax.ppermute(normed, "tp", ring)
+        owner = lax.rem(tp + n_tp - shift, n_tp)
+        span_rows = lax.dynamic_update_slice_in_dim(span_rows, moved, owner * rows, axis=0)
+    gate_hidden = jnp.dot(span_rows, gate_whole, preferred_element_type=jnp.float32)
+    up_hidden = jnp.dot(span_rows, up_whole, preferred_element_type=jnp.float32)
     hidden = (jax.nn.silu(gate_hidden) * up_hidden).astype(jnp.bfloat16)
-    channel_term = jnp.dot(
-        hidden, lax.all_gather(w_down, "sp", axis=1, tiled=True), preferred_element_type=jnp.float32
-    )
-    channel_sum = lax.psum_scatter(
-        channel_term.astype(jnp.bfloat16), "tp", scatter_dimension=0, tiled=True
-    ).astype(jnp.float32)
+    channel_term = jnp.concatenate(
+        [
+            jnp.dot(hidden, part, preferred_element_type=jnp.float32).astype(jnp.bfloat16)
+            for part in downs
+        ],
+        axis=1,
+    )
+    channel_sum = lax.psum_scatter(channel_term, "tp", scatter_dimension=0, tiled=True)
+    if w_down.shape[1] % 128 == 0:
+        return place(middle, channel_sum)
+    size, index = lax.axis_size("sp"), lax.axis_index("sp")
+    width = w_down.shape[1]
+    blocks = [
+        lax.dynamic_slice_in_dim(channel_sum, (index ^ owner) * width, width, axis=1)
+        for owner in range(size)
+    ]
+    channel_sum = jnp.concatenate(blocks, axis=1).astype(jnp.float32)
     return (middle_f + 0.5 * channel_sum).astype(jnp.bfloat16)
 
 
 def solution(mesh):
     return jax.shard_map(
-        per_device,
+        layer,
         mesh=mesh,
         in_specs=(
             P("sp", "tp"),

time: 506 us -> 336 us (0.66)
  waiting for transfers between devices: 397 us -> 149 us
  blocking collectives: 15.1 us -> 67.1 us
  starting transfers between devices: 0.24 us -> 15.3 us
  matrix products: 23.4 us -> 30.9 us
    all_gather x6 -> x2, waiting for transfers between devices: 368 us -> 17.6 us  [the longest x1 17.5 us: layer(): up_whole = lax.all_gather(w_up, 'sp', axis=0, tiled=True)]
    ppermute x0 -> x13, waiting for transfers between devices: none -> 95.3 us  [the longest x7 86.2 us: exchange_gather(): pieces[held ^ bit] = lax.ppermute(pieces[held], axis, pairs)]
    all_gather x0 -> x2, blocking collectives: none -> 67.1 us  [layer(): lax.all_gather(state[i * step:(i + 1) * step], 'sp')]
    all_to_all x1 -> x0, blocking collectives: 15.1 us -> none  [per_device(): lax.all_to_all(mixed_heads, 'tp', split_axis=0, concat_axis=1, tiled=True)]
    ppermute x0 -> x13, starting transfers between devices: none -> 11.7 us  [the longest x7 6.44 us: exchange_gather(): pieces[held ^ bit] = lax.ppermute(pieces[held], axis, pairs)]
    dot_general x3 -> x14, matrix products: 23.4 us -> 30.9 us  [the longest x8 11.6 us: layer(): jnp.dot(hidden, part, preferred_element_type=jnp.float32)]
    all_to_all x0 -> x1, waiting for transfers between devices: none -> 7.21 us  [layer(): lax.all_to_all(mixed_heads.reshape(n_tp, rows, mixed_heads.shape[1]), 'tp...]
  transfers between devices with their start and end apart: 7 -> 17, of which waited for: 7 -> 6; matrix products, arithmetic and copies ran while one was open for 3% -> 10% of each run, Pallas kernels for 1% -> 16%
where the time goes in v2:
time: 336 us; the launch traced here: 335 us
  waiting for transfers between devices  149 us (44%)
  blocking collectives  67.1 us (20%)
  Pallas kernels  54.8 us (16%)
  matrix products  30.9 us (9%)
  starting transfers between devices  15.3 us (5%)
  between operations  13.4 us (4%)
    ppermute x7, waiting for transfers between devices, exchange_gather(): pieces[held ^ bit] = lax.ppermute(pieces[held], axis, pairs)  86.2 us
    all_gather x2, blocking collectives, layer(): lax.all_gather(state[i * step:(i + 1) * step], 'sp')  67.1 us
    pallas_call x1, Pallas kernels, mixer(): pl.pallas_call(mixer_kernel, name='mixer', out_shape=(jax.ShapeDtypeStruc...  47.9 us
    reduce_scatter x1, waiting for transfers between devices, layer(): lax.psum_scatter(channel_term, 'tp', scatter_dimension=0, tiled=True)  27.1 us
    all_gather x1, waiting for transfers between devices, layer(): up_whole = lax.all_gather(w_up, 'sp', axis=0, tiled=True)  17.5 us
    dot_general x8, matrix products, layer(): jnp.dot(hidden, part, preferred_element_type=jnp.float32)  11.6 us
    ppermute x3, waiting for transfers between devices, layer(): moved = lax.ppermute(normed, 'tp', ring)  9.13 us
    all_to_all x1, waiting for transfers between devices, layer(): lax.all_to_all(mixed_heads.reshape(n_tp, rows, mixed_heads.shape[1]), 'tp...  7.21 us
  transfers between devices with their start and end apart: 17, of which 6 were waited for; matrix products, arithmetic and copies ran while one was open for 10% of the time, Pallas kernels for 16%

profile of v2, /device:TPU:0, one launch (start us, length us, event | category | flops | bytes accessed | tf_op | source)
XLA Modules:
  0.0 334.8 jit_solution(18197043953273139139)
XLA Ops:
  8.6 2.0 collective-permute-start.2
  10.5 2.2 collective-permute-start.1
  14.3 47.9 %mixer.1 = (bf16[4,128,128]{2,1,0:T(8,128)(2,1)}, f32[384,512]{1,0:T(8,128)}, bf16[384,512]{1,0:T(8,128)(2,1)}) custom-call(bf16[384,512]{1,0:T(8,128)(2,1)} %q_ref.1, bf16[384,512]{1,0:T(8,128)(2,1)} %k_ref.1, bf16[384,512]{1,0:T(8,128)(2,1)} %v_ref.1, f32[8,384]{1,0:T(8,128)} %beta_ref.1, f32[8,384]{1,0:T(8,128)} %decay_ref.1), custom_call_target="tpu_custom_call" | custom-call | flops 50331648000 | bytes 1572864 | tf_op jit(solution)/shard_map/mixer/pallas_call | solution.py:155
  63.2 34.3 %all-gather = bf16[16,128,128]{2,1,0:T(8,128)(2,1)S(1)} all-gather(bf16[2,128,128]{2,1,0:T(8,128)(2,1)S(1)} %get-tuple-element.13), channel_id=2, replica_groups=mesh['sp'=8,'tp'=4] {'sp'}, dimensions={0}, use_global_device_ids=true | all-gather | bytes 589824 | tf_op jit(solution)/shard_map/all_gather | solution.py:280
  97.5 32.8 %all-gather.1 = bf16[16,128,128]{2,1,0:T(8,128)(2,1)S(1)} all-gather(bf16[2,128,128]{2,1,0:T(8,128)(2,1)S(1)} %get-tuple-element.14), channel_id=3, replica_groups=mesh['sp'=8,'tp'=4] {'sp'}, dimensions={0}, use_global_device_ids=true | all-gather | bytes 589824 | tf_op jit(solution)/shard_map/all_gather | solution.py:280
  131.9 4.9 %finish.1 = bf16[384,512]{1,0:T(8,128)(2,1)} custom-call(bf16[8,4,128,128]{3,2,1,0:T(8,128)(2,1)} %pad_maximum_fusion.every_ref, f32[384,512]{1,0:T(8,128)} %get-tuple-element.9.local_ref, bf16[384,512]{1,0:T(8,128)(2,1)} %get-tuple-element.10.reach_ref, bf16[384,512]{1,0:T(8,128)(2,1)} %gates_ref.1, f32[1,128]{1,0:T(1,128)} %maximum_bitcast_fusion.gain_ref), custom_call_target="tpu_custom_call" | custom-call | flops 100663296 | bytes 1572864 | tf_op jit(solution)/shard_map/finish/pallas_call | solution.py:205
  136.9 3.5 %all-to-all-start = ((bf16[4,96,512]{2,1,0:T(8,128)(2,1)}), bf16[4,96,512]{2,1,0:T(8,128)(2,1)S(1)}, u32[]{:S(2)}, u32[]{:S(2)}) async-start(bf16[4,96,512]{2,1,0:T(8,128)(2,1)} %bitcast.45), calls=%async_computation | async-start | bytes 786432 | tf_op jit(solution)/shard_map/all_to_all | solution.py:284
  140.5 7.2 %all-to-all-done = bf16[4,96,512]{2,1,0:T(8,128)(2,1)S(1)} async-done(((bf16[4,96,512]{2,1,0:T(8,128)(2,1)}), bf16[4,96,512]{2,1,0:T(8,128)(2,1)S(1)}, u32[]{:S(2)}, u32[]{:S(2)}) %all-to-all-start) | async-done | bytes 393248 | tf_op jit(solution)/shard_map/all_to_all | solution.py:284
  147.7 2.1 fusion.18
  149.9 2.1 fusion.14
  152.0 2.1 convolution_add_fusion.1
  157.3 9.1 %collective-permute-done.3 = bf16[96,2048]{1,0:T(8,128)(2,1)S(1)} collective-permute-done((bf16[96,2048]{1,0:T(8,128)(2,1)S(1)}, bf16[96,2048]{1,0:T(8,128)(2,1)S(1)}, u32[]{:S(2)}, u32[]{:S(2)}) %collective-permute-start.3) | collective-permute-done | bytes 393248 | tf_op jit(solution)/shard_map/ppermute | solution.py:300
  166.5 44.9 %collective-permute-done.9 = bf16[1408,256]{1,0:T(8,128)(2,1)} collective-permute-done((bf16[1408,256]{1,0:T(8,128)(2,1)}, bf16[1408,256]{1,0:T(8,128)(2,1)}, u32[]{:S(2)}, u32[]{:S(2)}) %collective-permute-start.9) | collective-permute-done | bytes 720928 | tf_op jit(solution)/shard_map/ppermute | solution.py:224
  213.0 41.3 %collective-permute-done.11 = bf16[1408,256]{1,0:T(8,128)(2,1)} collective-permute-done((bf16[1408,256]{1,0:T(8,128)(2,1)}, bf16[1408,256]{1,0:T(8,128)(2,1)}, u32[]{:S(2)}, u32[]{:S(2)}) %collective-permute-start.11) | collective-permute-done | bytes 720928 | tf_op jit(solution)/shard_map/ppermute | solution.py:224
  256.4 6.6 %fusion.30 = f32[384,1408]{1,0:T(8,128)} fusion(bf16[384,2048]{1,0:T(8,128)(2,1)S(1)} %constant_dynamic-update-slice_fusion, bf16[2048,1408]{1,0:T(8,128)(2,1)} %all-gather.5.cloned.1.call-done), kind=kOutput, calls=%fused_computation.49 | convolution fusion | flops 2214592512 | bytes 9502720 | tf_op jit(solution)/shard_map/dot_general | solution.py:303
  263.0 17.5 %all-gather.7.cloned.1.call-done = bf16[2048,1408]{1,0:T(8,128)(2,1)} async-done(((bf16[256,1408]{1,0:T(8,128)(2,1)}), bf16[2048,1408]{1,0:T(8,128)(2,1)}) %all-gather.7.cloned.1.call-update) | async-done | bytes 5767184 | tf_op jit(solution)/shard_map/all_gather | solution.py:269
  280.5 5.8 %multiply_convert_fusion = bf16[384,1408]{1,0:T(8,128)(2,1)S(1)} fusion(f32[384,1408]{1,0:T(8,128)} %fusion.30, bf16[384,2048]{1,0:T(8,128)(2,1)S(1)} %constant_dynamic-update-slice_fusion, bf16[2048,1408]{1,0:T(8,128)(2,1)} %all-gather.7.cloned.1.call-done), kind=kOutput, calls=%fused_computation.5 | convolution fusion | flops 2217836544 | bytes 10584064 | tf_op jit(solution)/shard_map/dot_general | solution.py:304
  286.4 1.6 fusion.10
  288.0 1.6 fusion.9
  292.7 1.6 fusion.6
  294.3 1.6 fusion.5
  295.9 1.6 fusion.4
  299.2 27.1 %reduce-scatter.2.cloned.1.call-done.sums_ref = bf16[96,2048]{1,0:T(8,128)(2,1)} async-done(((bf16[384,2048]{1,0:T(8,128)(2,1)}), bf16[96,2048]{1,0:T(8,128)(2,1)}) %reduce-scatter.2.cloned.1.call-update) | async-done | bytes 393232 | tf_op jit(solution)/shard_map/reduce_scatter | solution.py:313
  326.3 2.0 place.1
  (51 shorter events, 18.0 us)
Async XLA Ops:
  6.5 249.8 %all-gather.5.cloned.1.call-start = ((), (), s32[]{:S(2)}) async-start(), calls=%async_computation.2 | async-start | bytes 6488064 | tf_op jit(solution)/shard_map/all_gather | solution.py:268
  7.3 273.3 %all-gather.7.cloned.1.call-start = ((), (), s32[]{:S(2)}) async-start(), calls=%async_computation.3 | async-start | bytes 6488064 | tf_op jit(solution)/shard_map/all_gather | solution.py:269
  8.0 143.9 %collective-permute-start = (bf16[512,2048]{1,0:T(8,128)(2,1)}, bf16[512,2048]{1,0:T(8,128)(2,1)}, u32[]{:S(2)}, u32[]{:S(2)}) collective-permute-start(bf16[512,2048]{1,0:T(8,128)(2,1)} %param.20), channel_id=1, source_target_pairs={{0,1},{1,2},{2,3},{3,0},{4,5},{5,6},{6,7},{7,4},{8,9},{9,10},{10,1... | collective-permute-start | bytes 6291464 | tf_op jit(solution)/shard_map/ppermute | solution.py:273
  8.6 141.3 %collective-permute-start.2 = (bf16[512,2048]{1,0:T(8,128)(2,1)}, bf16[512,2048]{1,0:T(8,128)(2,1)}, u32[]{:S(2)}, u32[]{:S(2)}) collective-permute-start(bf16[512,2048]{1,0:T(8,128)(2,1)} %param.20), channel_id=1, source_target_pairs={{0,3},{1,0},{2,1},{3,2},{4,7},{5,4},{6,5},{7,6},{8,11},{9,8},{10,9... | collective-permute-start | bytes 6291464 | tf_op jit(solution)/shard_map/ppermute | solution.py:273
  10.5 143.5 %collective-permute-start.1 = (bf16[512,2048]{1,0:T(8,128)(2,1)}, bf16[512,2048]{1,0:T(8,128)(2,1)S(1)}, u32[]{:S(2)}, u32[]{:S(2)}) collective-permute-start(bf16[512,2048]{1,0:T(8,128)(2,1)} %param.20), channel_id=1, source_target_pairs={{0,2},{1,3},{2,0},{3,1},{4,6},{5,7},{6,4},{7,5},{8,10},{9,11},{10,... | collective-permute-start | bytes 6291464 | tf_op jit(solution)/shard_map/ppermute | solution.py:273
  12.8 137.0 %collective-permute-start.7 = (bf16[1408,256]{1,0:T(8,128)(2,1)}, bf16[1408,256]{1,0:T(8,128)(2,1)}, u32[]{:S(2)}, u32[]{:S(2)}) collective-permute-start(bf16[1408,256]{1,0:T(8,128)(2,1)} %param.25), channel_id=1, source_target_pairs={{0,8},{4,12},{8,0},{12,4},{16,24},{20,28},{24,16},{28,20},{1,9},{5... | collective-permute-start | bytes 2162696 | tf_op jit(solution)/shard_map/ppermute | solution.py:224
  63.1 68.2 %copy-start.4 = (f32[64]{0:T(128)S(1)}, f32[64]{0:T(128)}, u32[]{:S(2)}) copy-start(f32[64]{0:T(128)} %param.19) | copy-start | bytes 772
  136.9 10.8 %all-to-all-start = ((bf16[4,96,512]{2,1,0:T(8,128)(2,1)}), bf16[4,96,512]{2,1,0:T(8,128)(2,1)S(1)}, u32[]{:S(2)}, u32[]{:S(2)}) async-start(bf16[4,96,512]{2,1,0:T(8,128)(2,1)} %bitcast.45), calls=%async_computation | async-start | bytes 786432 | tf_op jit(solution)/shard_map/all_to_all | solution.py:284
  140.3 186.0 %reduce-scatter.2.cloned.1.call-start = ((), (), s32[]{:S(2)}) async-start(), calls=%async_computation.4 | async-start | bytes 1966080 | tf_op jit(solution)/shard_map/reduce_scatter | solution.py:313
  140.4 71.0 %collective-permute-start.9 = (bf16[1408,256]{1,0:T(8,128)(2,1)}, bf16[1408,256]{1,0:T(8,128)(2,1)}, u32[]{:S(2)}, u32[]{:S(2)}) collective-permute-start(bf16[1408,256]{1,0:T(8,128)(2,1)} %param.25), channel_id=1, source_target_pairs={{0,16},{4,20},{8,24},{12,28},{16,0},{20,4},{24,8},{28,12},{1,17},{... | collective-permute-start | bytes 2162696 | tf_op jit(solution)/shard_map/ppermute | solution.py:224
  149.8 104.5 %collective-permute-start.11 = (bf16[1408,256]{1,0:T(8,128)(2,1)}, bf16[1408,256]{1,0:T(8,128)(2,1)}, u32[]{:S(2)}, u32[]{:S(2)}) collective-permute-start(bf16[1408,256]{1,0:T(8,128)(2,1)} %collective-permute-done.7), channel_id=1, source_target_pairs={{0,16},{4,20},{8,24},{12,28},{16,0},{20,4},{24,8},{28,12},{1,17},{... | collective-permute-start | bytes 2162696 | tf_op jit(solution)/shard_map/ppermute | solution.py:224
  151.9 2.2 copy-start.2
  154.8 11.7 %copy-start = (bf16[96,2048]{1,0:T(8,128)(2,1)}, bf16[96,2048]{1,0:T(8,128)(2,1)S(1)}, u32[]{:S(2)}) copy-start(bf16[96,2048]{1,0:T(8,128)(2,1)S(1)} %get-tuple-element.16.middle_ref) | copy-start | bytes 1179652
  154.8 0.7 copy-start.3
  155.7 10.8 %collective-permute-start.3 = (bf16[96,2048]{1,0:T(8,128)(2,1)S(1)}, bf16[96,2048]{1,0:T(8,128)(2,1)S(1)}, u32[]{:S(2)}, u32[]{:S(2)}) collective-permute-start(bf16[96,2048]{1,0:T(8,128)(2,1)S(1)} %get-tuple-element.12), channel_id=1, source_target_pairs={{0,1},{1,2},{2,3},{3,0},{4,5},{5,6},{6,7},{7,4},{8,9},{9,10},{10,1... | collective-permute-start | bytes 1179656 | tf_op jit(solution)/shard_map/ppermute | solution.py:300
  155.7 100.0 %collective-permute-start.4 = (bf16[96,2048]{1,0:T(8,128)(2,1)S(1)}, bf16[96,2048]{1,0:T(8,128)(2,1)S(1)}, u32[]{:S(2)}, u32[]{:S(2)}) collective-permute-start(bf16[96,2048]{1,0:T(8,128)(2,1)S(1)} %get-tuple-element.12), channel_id=1, source_target_pairs={{0,2},{1,3},{2,0},{3,1},{4,6},{5,7},{6,4},{7,5},{8,10},{9,11},{10,... | collective-permute-start | bytes 1179656 | tf_op jit(solution)/shard_map/ppermute | solution.py:300
  156.2 131.8 %collective-permute-start.6 = (bf16[1408,256]{1,0:T(8,128)(2,1)}, bf16[1408,256]{1,0:T(8,128)(2,1)}, u32[]{:S(2)}, u32[]{:S(2)}) collective-permute-start(bf16[1408,256]{1,0:T(8,128)(2,1)} %param.25), channel_id=1, source_target_pairs={{0,4},{4,0},{8,12},{12,8},{16,20},{20,16},{24,28},{28,24},{1,5},{5... | collective-permute-start | bytes 2162696 | tf_op jit(solution)/shard_map/ppermute | solution.py:224
  166.5 89.8 %collective-permute-start.5 = (bf16[96,2048]{1,0:T(8,128)(2,1)S(1)}, bf16[96,2048]{1,0:T(8,128)(2,1)S(1)}, u32[]{:S(2)}, u32[]{:S(2)}) collective-permute-start(bf16[96,2048]{1,0:T(8,128)(2,1)S(1)} %get-tuple-element.12), channel_id=1, source_target_pairs={{0,3},{1,0},{2,1},{3,2},{4,7},{5,4},{6,5},{7,6},{8,11},{9,8},{10,9... | collective-permute-start | bytes 1179656 | tf_op jit(solution)/shard_map/ppermute | solution.py:300
  211.4 79.7 %collective-permute-start.8 = (bf16[1408,256]{1,0:T(8,128)(2,1)}, bf16[1408,256]{1,0:T(8,128)(2,1)}, u32[]{:S(2)}, u32[]{:S(2)}) collective-permute-start(bf16[1408,256]{1,0:T(8,128)(2,1)} %collective-permute-done.7), channel_id=1, source_target_pairs={{0,4},{4,0},{8,12},{12,8},{16,20},{20,16},{24,28},{28,24},{1,5},{5... | collective-permute-start | bytes 2162696 | tf_op jit(solution)/shard_map/ppermute | solution.py:224
  254.2 40.1 %collective-permute-start.10 = (bf16[1408,256]{1,0:T(8,128)(2,1)}, bf16[1408,256]{1,0:T(8,128)(2,1)}, u32[]{:S(2)}, u32[]{:S(2)}) collective-permute-start(bf16[1408,256]{1,0:T(8,128)(2,1)} %collective-permute-done.9), channel_id=1, source_target_pairs={{0,4},{4,0},{8,12},{12,8},{16,20},{20,16},{24,28},{28,24},{1,5},{5... | collective-permute-start | bytes 2162696 | tf_op jit(solution)/shard_map/ppermute | solution.py:224
  255.7 41.8 %collective-permute-start.12 = (bf16[1408,256]{1,0:T(8,128)(2,1)}, bf16[1408,256]{1,0:T(8,128)(2,1)S(1)}, u32[]{:S(2)}, u32[]{:S(2)}) collective-permute-start(bf16[1408,256]{1,0:T(8,128)(2,1)} %collective-permute-done.11), channel_id=1, source_target_pairs={{0,4},{4,0},{8,12},{12,8},{16,20},{20,16},{24,28},{28,24},{1,5},{5... | collective-permute-start | bytes 2162696 | tf_op jit(solution)/shard_map/ppermute | solution.py:224
  298.0 1.2 copy-start.1
Sparse Core Ops, SparseCore 0:
  9.5 119.1 all-gather.4
  130.9 149.5 all-gather.6
  299.3 26.9 reduce-scatter.1
